TPU v7x, 32 devices: a whole 2x2x4 slice. The times are simulated.
32 devices in a mesh: ep: 16 (over z, y, core), tp: 2 (over x).
Axes of the slice: x: 2, y: 2, z: 4, core: 2. Of those that a mesh axis runs over, the one named last changes fastest.
Arguments:
- residual_in: bfloat16 [320, 1024], P('ep', 'tp'), may hold values from -64 to 64
- queries: bfloat16 [320, 512], P(('ep', 'tp')), may hold values from -6 to 6
- cache_keys: bfloat16 [320, 1024, 128], P(('ep', 'tp')), may hold values from -6 to 6
- cache_values: bfloat16 [320, 1024, 128], P(('ep', 'tp')), may hold values from -24 to 24
- lengths: int32 [320], P(('ep', 'tp')), may hold values from 256 to 1024
- stick_offset: float32 [8], replicated, may hold values from 0.5 to 6
- out_weight: bfloat16 [512, 1024], P(None, 'tp'), may hold values from -0.25 to 0.25
- norm1_gain: float32 [1024], P('tp'), may hold values from 0.3 to 3.1
- norm1_bias: float32 [1024], P('tp'), may hold values from -1.5 to 1.5
- routes: int32 [320, 6], P('ep'), may hold values from 0 to 15, all different within a row; in each aligned block of 20 rows (0 to 19, 20 to 39, ...) at most 16 rows name the same one
- route_weights: float32 [320, 6], P('ep'), may hold values from 0.1 to 0.8
- expert_gate: bfloat16 [16, 1024, 512], P('ep', None, 'tp'), may hold values from -0.1875 to 0.1875
- expert_up: bfloat16 [16, 1024, 512], P('ep', None, 'tp'), may hold values from -0.1875 to 0.1875
- expert_down: bfloat16 [16, 512, 1024], P('ep', 'tp'), may hold values from -0.25 to 0.25
- shared_gate: bfloat16 [1024, 512], P(None, 'tp'), may hold values from -0.1875 to 0.1875
- shared_up: bfloat16 [1024, 512], P(None, 'tp'), may hold values from -0.1875 to 0.1875
- shared_down: bfloat16 [512, 1024], P('tp'), may hold values from -0.25 to 0.25
- norm2_gain: float32 [1024], P('tp'), may hold values from 0.1 to 1.9
- norm2_bias: float32 [1024], P('tp'), may hold values from -1.5 to 1.5
Outputs:
- layer_out: bfloat16 [320, 1024], P('ep', 'tp')
Inputs may be any that keep to these rules, and one draw needn't show every extreme that they name: `routes`: each row names 6 different experts; among the rows of one index of ep no expert is named more than 16 times.
All inputs are finite; a program needn't handle non-finite values.
Results may differ from a plain program's by a relative error of at most 0.0095.
Values may be sent and summed in bfloat16 or wider, within the bound.
A program may use at most 64 MiB of HBM per device.

v0:
```python
import jax
import jax.numpy as jnp
from jax import lax
from jax.sharding import PartitionSpec as P

H = 8
HD = 64
KVH = 2
CACHE = 1024
TOPK = 6


RESIDUAL_SCALE = 2.0**0.25
EPSILON = 1e-05


def normalize(totals, squares, entries, values, scales, shifts):
    centre = totals / entries
    spread = squares / entries - centre * centre
    return (values - centre) * lax.rsqrt(spread + EPSILON) * scales + shifts


def stick_read(queries, keys_block, values_block, lengths, offsets):
    seq_count = queries.shape[0]
    grouped = H // KVH
    query_heads = queries.reshape(seq_count, KVH, grouped, HD)
    key_heads = keys_block.reshape(seq_count, CACHE, KVH, HD)
    value_heads = values_block.reshape(seq_count, CACHE, KVH, HD)
    scores = jnp.einsum(
        "sgjd,slgd->sgjl", query_heads, key_heads, preferred_element_type=jnp.float32
    )
    scores = scores * HD ** (-0.5) - offsets.reshape(1, KVH, grouped, 1)
    live_mask = (jnp.arange(CACHE)[None, :] < lengths[:, None])[:, None, None, :]
    keep_log = jnp.where(live_mask, jax.nn.log_sigmoid(-scores), 0.0)
    after_log = lax.cumsum(keep_log, axis=3, reverse=True) - keep_log
    weights = jnp.where(live_mask, jnp.exp(jax.nn.log_sigmoid(scores) + after_log), 0.0)
    weights = weights.astype(jnp.bfloat16)
    mixed = jnp.einsum("sgjl,slgd->sgjd", weights, value_heads, preferred_element_type=jnp.float32)
    return mixed.reshape(seq_count, H * HD).astype(jnp.bfloat16)


def body(
    residual_in,
    queries,
    cache_keys,
    cache_values,
    lengths,
    stick_offset,
    out_weight,
    norm1_gain,
    norm1_bias,
    routes,
    route_weights,
    expert_gate,
    expert_up,
    expert_down,
    shared_gate,
    shared_up,
    shared_down,
    norm2_gain,
    norm2_bias,
):
    mixed = stick_read(queries, cache_keys, cache_values, lengths, stick_offset)
    attended = jnp.dot(
        lax.all_gather(mixed, "tp", axis=0, tiled=True),
        out_weight,
        preferred_element_type=jnp.float32,
    )
    before = RESIDUAL_SCALE * residual_in.astype(jnp.float32) + attended
    group_rows, columns = residual_in.shape
    full_width = columns * lax.axis_size("tp")
    totals, squares = lax.psum((jnp.sum(before, axis=1), jnp.sum(before * before, axis=1)), "tp")
    normed = normalize(
        totals[:, None], squares[:, None], full_width, before, norm1_gain, norm1_bias
    ).astype(jnp.bfloat16)
    whole = lax.all_gather(normed, "tp", axis=1, tiled=True)
    experts = lax.axis_size("ep")
    capacity = min(group_rows, 2 * ((group_rows * TOPK + experts - 1) // experts))
    slots_all = experts * capacity
    chosen = routes.reshape(-1)
    order_ids = jnp.arange(chosen.shape[0])
    matches = (chosen[:, None] == chosen[None, :]) & (order_ids[None, :] < order_ids[:, None])
    targets = chosen * capacity + jnp.sum(matches.astype(jnp.int32), axis=1)
    picks = (targets[:, None] == jnp.arange(slots_all)[None, :]).astype(jnp.float32)
    picks = picks.reshape(group_rows, TOPK, slots_all)
    dispatch = jnp.sum(picks, axis=1).astype(jnp.bfloat16)
    combine = jnp.sum(picks * route_weights[:, :, None], axis=1)
    parcel = jnp.einsum("sr,sd->rd", dispatch, normed, preferred_element_type=jnp.float32)
    parcel = parcel.astype(jnp.bfloat16).reshape(experts, capacity, columns)
    arrived = lax.all_gather(
        lax.all_to_all(parcel, "ep", split_axis=0, concat_axis=0, tiled=True),
        "tp",
        axis=2,
        tiled=True,
    )
    gate_part = jnp.einsum(
        "ecd,df->ecf", arrived, expert_gate[0], preferred_element_type=jnp.float32
    )
    up_part = jnp.einsum("ecd,df->ecf", arrived, expert_up[0], preferred_element_type=jnp.float32)
    hidden = (jax.nn.silu(gate_part) * up_part).astype(jnp.bfloat16)
    partial_value = jnp.einsum(
        "ecf,fd->ecd", hidden, expert_down[0], preferred_element_type=jnp.float32
    )
    summed = lax.psum_scatter(
        partial_value.astype(jnp.bfloat16), "tp", scatter_dimension=2, tiled=True
    )
    returned = lax.all_to_all(summed, "ep", split_axis=0, concat_axis=0, tiled=True)
    routed = jnp.dot(
        combine,
        returned.reshape(slots_all, columns).astype(jnp.float32),
        precision=lax.Precision.HIGHEST,
    )
    shared_hidden = (
        jax.nn.silu(jnp.dot(whole, shared_gate, preferred_element_type=jnp.float32))
        * jnp.dot(whole, shared_up, preferred_element_type=jnp.float32)
    ).astype(jnp.bfloat16)
    shared_term = jnp.dot(shared_hidden, shared_down, preferred_element_type=jnp.float32)
    shared = lax.psum_scatter(
        shared_term.astype(jnp.bfloat16), "tp", scatter_dimension=1, tiled=True
    ).astype(jnp.float32)
    after = RESIDUAL_SCALE * normed.astype(jnp.float32) + routed + shared
    final_totals, final_squares = lax.psum(
        (jnp.sum(after, axis=1), jnp.sum(after * after, axis=1)), "tp"
    )
    return normalize(
        final_totals[:, None], final_squares[:, None], full_width, after, norm2_gain, norm2_bias
    ).astype(jnp.bfloat16)


def solution(mesh):
    in_specs = (
        P("ep", "tp"),
        P(("ep", "tp"), None),
        P(("ep", "tp"), None, None),
        P(("ep", "tp"), None, None),
        P(("ep", "tp")),
        P(),
        P(None, "tp"),
        P("tp"),
        P("tp"),
        P("ep", None),
        P("ep", None),
        P("ep", None, "tp"),
        P("ep", None, "tp"),
        P("ep", "tp", None),
        P(None, "tp"),
        P(None, "tp"),
        P("tp", None),
        P("tp"),
        P("tp"),
    )
    out_specs = P("ep", "tp")
    return jax.shard_map(body, mesh=mesh, in_specs=in_specs, out_specs=out_specs, check_vma=False)
```

profile of v0, /device:TPU:0, one launch (start us, length us, event | category | flops | bytes accessed | tf_op | source)
XLA Modules:
  0.0 211.8 jit_solution(5115678477667394702)
XLA Ops:
  6.5 0.0 copy-start
  6.5 0.0 reduce-scatter.3.cloned.1.call-start
  6.5 0.8 iota_compare_fusion.1
  7.3 0.0 copy-start.8
  7.3 0.0 copy-start.16
  7.4 4.5 %copy.46 = bf16[10,1024,128]{1,2,0:T(8,128)(2,1)} copy(bf16[10,1024,128]{2,1,0:T(8,128)(2,1)} %param.21) | data formatting | bytes 5242880 | tf_op args[2]
  11.9 0.0 copy-done.8
  11.9 0.1 reshape.87
  12.0 0.0 copy-done.16
  12.0 0.1 sub.37
  12.1 3.3 %fusion.15 = (f32[10,2,4,1024]{3,2,1,0:T(4,128)S(1)}, f32[10,2,4,1024]{3,2,1,0:T(4,128)}) fusion(pred[10,1024]{1,0:T(8,128)(4,1)S(1)} %iota_compare_fusion.1, f32[2,4]{1,0:T(2,128)S(1)} %sub.37, bf16[10,2,4,64]{3,2,1,0:T(4,128)(2,1)S(1)} %reshape.87, bf16[10,1024,2,64]{1,3,2,0:T(8,128)(2,1)} %bitcast.38), kind=kOutput, calls=%fused_computation.25 | convolution fusion | flops 11304960 | bytes 3297312 | tf_op jit(solution)/shard_map/sgjd,slgd->sgjl/dot_general | solution.py:29
  15.4 0.8 reshape.89
  16.2 99.6 %reduce-window.6 = f32[10,2,4,8,128]{4,3,2,1,0:T(8,128)S(1)} reduce-window(f32[10,2,4,8,128]{4,3,2,1,0:T(8,128)} %reshape.89, f32[]{:T(128)} %constant.24.clone.1), window={size=1x1x1x1x128 pad=0_0x0_0x0_0x0_0x0_127}, to_apply=%region_0.1 | reduce-window | flops 10403840 | bytes 655364 | tf_op jit(solution)/shard_map/reduce-window
  115.8 1.1 copy.47
  116.9 0.8 reduce-window.9
  117.7 0.6 slice.9
  118.3 0.9 copy.48
  119.2 0.9 broadcast_add_fusion
  120.1 1.1 reduce_window_sum.15
  121.1 0.0 copy-done.1
  121.2 2.7 %copy.49 = bf16[10,1024,128]{1,2,0:T(8,128)(2,1)} copy(bf16[10,1024,128]{2,1,0:T(8,128)(2,1)S(1)} %copy-done.1) | data formatting | bytes 5242880 | tf_op args[3]
  123.9 0.0 copy-start.11
  123.9 0.0 copy-start.12
  123.9 3.0 %convolution_convert_fusion.3 = bf16[10,2,4,64]{3,2,1,0:T(4,128)(2,1)S(1)} fusion(bf16[10,1024,2,64]{1,3,2,0:T(8,128)(2,1)} %bitcast.39, f32[10,2,4,1024]{3,2,1,0:T(4,128)S(1)} %reduce_window_sum.15, f32[10,2,4,1024]{3,2,1,0:T(4,128)} %get-tuple-element.20, pred[10,1024]{1,0:T(8,128)(4,1)S(1)} %iota_compare_fusion.1), kind=kOutput, calls=%fused_computation.10 | convolution fusion | flops 12129280 | bytes 3297280 | tf_op jit(solution)/shard_map/sgjl,slgd->sgjd/dot_general | solution.py:38
  126.9 0.1 reshape.94
  127.0 5.5 %all-gather = bf16[2,10,512]{2,1,0:T(8,128)(2,1)S(1)} all-gather(bf16[1,10,512]{2,1,0:T(8,128)(2,1)S(1)} %reshape.94), channel_id=1, replica_groups=mesh['ep'=16,'tp'=2] {'tp'}, dimensions={0}, use_global_device_ids=true | all-gather | bytes 30720 | tf_op jit(solution)/shard_map/all_gather | solution.py:65
  132.5 0.0 copy-done.9
  132.5 0.1 copy.50
  132.6 0.1 eq.29
  132.7 0.2 convert_reduce_fusion.1
  132.9 0.1 reduce_sum.68
  133.0 0.1 copy.51
  133.1 0.0 copy-done.2
  133.1 0.0 copy-done.7
  133.1 0.3 fusion.38
  133.4 4.9 %all-reduce.1 = (f32[20]{0:T(128)S(1)}, f32[20]{0:T(128)S(1)}) all-reduce(f32[20]{0:T(128)S(1)} %get-tuple-element.8, f32[20]{0:T(128)S(1)} %get-tuple-element.7), channel_id=1, replica_groups=mesh['ep'=16,'tp'=2] {'tp'}, use_global_device_ids=true, to_apply=%region_5.6 | all-reduce | flops 40 | bytes 320 | tf_op jit(solution)/shard_map/psum | solution.py:72
  138.4 0.0 copy-done.10
  138.4 0.1 convert_reduce_fusion
  138.5 0.0 copy-done.11
  138.5 0.0 copy-done.12
  138.5 0.1 add_convert_fusion.1
  138.6 0.3 convolution_convert_fusion.1
  138.8 16.3 %all_to_all.10 = bf16[16,16,512]{2,1,0:T(8,128)(2,1)S(1)} all-to-all(bf16[16,16,512]{2,1,0:T(8,128)(2,1)S(1)} %bitcast.41), channel_id=1, replica_groups=mesh['ep'=16,'tp'=2] {'ep'}, dimensions={0} | all-to-all | bytes 524288 | tf_op jit(solution)/shard_map/all_to_all | solution.py:91
  155.1 8.8 %all_gather.10 = bf16[16,16,1024]{2,1,0:T(8,128)(2,1)S(1)} all-gather(bf16[16,16,512]{2,1,0:T(8,128)(2,1)S(1)} %all_to_all.10), channel_id=1, replica_groups=mesh['ep'=16,'tp'=2] {'tp'}, dimensions={2}, use_global_device_ids=true | all-gather | bytes 786432 | tf_op jit(solution)/shard_map/all_gather | solution.py:90
  163.9 0.3 fusion.7
  164.2 0.0 copy-start.5
  164.3 0.0 copy-start.6
  164.3 0.0 copy-start.13
  164.3 0.0 copy-start.14
  164.3 1.5 convolution_convert_fusion
  165.8 0.0 reduce-scatter.3.cloned.1.call-update
  165.9 4.5 %all_gather.11 = bf16[20,1024]{1,0:T(8,128)(2,1)S(1)} all-gather(bf16[20,512]{1,0:T(8,128)(2,1)S(1)} %add_convert_fusion.1), channel_id=1, replica_groups=mesh['ep'=16,'tp'=2] {'tp'}, dimensions={1}, use_global_device_ids=true | all-gather | bytes 61440 | tf_op jit(solution)/shard_map/all_gather | solution.py:76
  170.4 8.8 %reduce-scatter.3.cloned.1.call-done = bf16[16,16,512]{2,1,0:T(8,128)(2,1)} async-done(((bf16[16,16,1024]{2,1,0:T(8,128)(2,1)}), bf16[16,16,512]{2,1,0:T(8,128)(2,1)}) %reduce-scatter.3.cloned.1.call-update) | async-done | bytes 262160 | tf_op jit(solution)/shard_map/reduce_scatter | solution.py:104
  179.2 5.6 %all-to-all-start.1 = ((bf16[16,16,512]{2,1,0:T(8,128)(2,1)}), bf16[16,16,512]{2,1,0:T(8,128)(2,1)S(1)}, u32[]{:S(2)}, u32[]{:S(2)}) async-start(bf16[16,16,512]{2,1,0:T(8,128)(2,1)} %reduce-scatter.3.cloned.1.call-done), calls=%async_computation.2 | async-start | bytes 524288 | tf_op jit(solution)/shard_map/all_to_all | solution.py:107
  184.8 0.0 reduce-scatter.5.cloned.1.call-start
  184.9 0.2 fusion.39
  185.1 0.0 copy-done.5
  185.1 1.1 convolution_convert_fusion.2
  186.2 0.0 reduce-scatter.5.cloned.1.call-update
  186.2 12.0 %reduce-scatter.5.cloned.1.call-done = bf16[20,512]{1,0:T(8,128)(2,1)} async-done(((bf16[20,1024]{1,0:T(8,128)(2,1)}), bf16[20,512]{1,0:T(8,128)(2,1)}) %reduce-scatter.5.cloned.1.call-update) | async-done | bytes 20496 | tf_op jit(solution)/shard_map/reduce_scatter | solution.py:118
  198.3 0.0 all-to-all-done.1
  198.3 1.1 fusion.37
  199.3 4.9 %all-reduce = (f32[20]{0:T(128)S(1)}, f32[20]{0:T(128)S(1)}) all-reduce(f32[20]{0:T(128)S(1)} %get-tuple-element.6, f32[20]{0:T(128)S(1)} %get-tuple-element.5), channel_id=1, replica_groups=mesh['ep'=16,'tp'=2] {'tp'}, use_global_device_ids=true, to_apply=%region_14.15 | all-reduce | flops 40 | bytes 320 | tf_op jit(solution)/shard_map/psum | solution.py:122
  204.3 0.7 add_convert_fusion
  (19 shorter events, 0.1 us)
Async XLA Ops:
  6.5 157.7 %copy-start = (bf16[1,256,1024]{2,1,0:T(8,128)(2,1)S(1)}, bf16[1,256,1024]{2,1,0:T(8,128)(2,1)}, u32[]{:S(2)}) copy-start(bf16[1,256,1024]{2,1,0:T(8,128)(2,1)} %param.32) | copy-start | bytes 1572868
  6.5 172.7 %reduce-scatter.3.cloned.1.call-start = ((), (), s32[]{:S(2)}) async-start(), calls=%async_computation.4 | async-start | bytes 786432 | tf_op jit(solution)/shard_map/reduce_scatter | solution.py:104
  7.3 4.6 %copy-start.8 = (bf16[10,512]{1,0:T(8,128)(2,1)S(1)}, bf16[10,512]{1,0:T(8,128)(2,1)}, u32[]{:S(2)}) copy-start(bf16[10,512]{1,0:T(8,128)(2,1)} %param.20) | copy-start | bytes 30724
  7.3 4.7 %copy-start.16 = (f32[8]{0:T(128)S(1)}, f32[8]{0:T(128)}, u32[]{:S(2)}) copy-start(f32[8]{0:T(128)} %param.24) | copy-start | bytes 100
  12.1 109.1 %copy-start.1 = (bf16[10,1024,128]{2,1,0:T(8,128)(2,1)S(1)}, bf16[10,1024,128]{2,1,0:T(8,128)(2,1)}, u32[]{:S(2)}) copy-start(bf16[10,1024,128]{2,1,0:T(8,128)(2,1)} %param.22) | copy-start | bytes 7864324
  123.9 8.6 %copy-start.9 = (s32[20,6]{0,1:T(8,128)S(1)}, s32[20,6]{0,1:T(8,128)}, u32[]{:S(2)}) copy-start(s32[20,6]{0,1:T(8,128)} %param.28) | copy-start | bytes 1444
  123.9 9.2 %copy-start.2 = (bf16[512,512]{1,0:T(8,128)(2,1)S(1)}, bf16[512,512]{1,0:T(8,128)(2,1)}, u32[]{:S(2)}) copy-start(bf16[512,512]{1,0:T(8,128)(2,1)} %param.25) | copy-start | bytes 1572868
  123.9 9.2 %copy-start.7 = (bf16[20,512]{1,0:T(8,128)(2,1)S(1)}, bf16[20,512]{1,0:T(8,128)(2,1)}, u32[]{:S(2)}) copy-start(bf16[20,512]{1,0:T(8,128)(2,1)} %param.19) | copy-start | bytes 61444
  123.9 14.5 %copy-start.10 = (f32[20,6]{0,1:T(8,128)S(1)}, f32[20,6]{0,1:T(8,128)}, u32[]{:S(2)}) copy-start(f32[20,6]{0,1:T(8,128)} %param.29) | copy-start | bytes 1444
  123.9 14.6 %copy-start.11 = (f32[512]{0:T(512)S(1)}, f32[512]{0:T(512)}, u32[]{:S(2)}) copy-start(f32[512]{0:T(512)} %param.27) | copy-start | bytes 6148
  123.9 14.6 %copy-start.12 = (f32[512]{0:T(512)S(1)}, f32[512]{0:T(512)}, u32[]{:S(2)}) copy-start(f32[512]{0:T(512)} %param.26) | copy-start | bytes 6148
  126.9 37.0 %copy-start.4 = (bf16[1,1024,256]{2,1,0:T(8,128)(2,1)S(1)}, bf16[1,1024,256]{2,1,0:T(8,128)(2,1)}, u32[]{:S(2)}) copy-start(bf16[1,1024,256]{2,1,0:T(8,128)(2,1)} %param.30) | copy-start | bytes 1572868
  126.9 37.3 %copy-start.15 = (bf16[1,1024,256]{2,1,0:T(8,128)(2,1)S(1)}, bf16[1,1024,256]{2,1,0:T(8,128)(2,1)}, u32[]{:S(2)}) copy-start(bf16[1,1024,256]{2,1,0:T(8,128)(2,1)} %param.31) | copy-start | bytes 1572868
  163.9 21.0 %copy-start.3 = (bf16[1024,256]{1,0:T(8,128)(2,1)S(1)}, bf16[1024,256]{1,0:T(8,128)(2,1)}, u32[]{:S(2)}) copy-start(bf16[1024,256]{1,0:T(8,128)(2,1)} %param.33) | copy-start | bytes 1572868
  164.2 20.8 %copy-start.5 = (bf16[256,1024]{1,0:T(8,128)(2,1)S(1)}, bf16[256,1024]{1,0:T(8,128)(2,1)}, u32[]{:S(2)}) copy-start(bf16[256,1024]{1,0:T(8,128)(2,1)} %param.35) | copy-start | bytes 1572868
  164.3 20.8 %copy-start.6 = (bf16[1024,256]{1,0:T(8,128)(2,1)S(1)}, bf16[1024,256]{1,0:T(8,128)(2,1)}, u32[]{:S(2)}) copy-start(bf16[1024,256]{1,0:T(8,128)(2,1)} %param.34) | copy-start | bytes 1572868
  164.3 40.0 %copy-start.13 = (f32[512]{0:T(512)S(1)}, f32[512]{0:T(512)}, u32[]{:S(2)}) copy-start(f32[512]{0:T(512)} %param.37) | copy-start | bytes 6148
  164.3 40.0 %copy-start.14 = (f32[512]{0:T(512)S(1)}, f32[512]{0:T(512)}, u32[]{:S(2)}) copy-start(f32[512]{0:T(512)} %param.36) | copy-start | bytes 6148
  179.2 19.1 %all-to-all-start.1 = ((bf16[16,16,512]{2,1,0:T(8,128)(2,1)}), bf16[16,16,512]{2,1,0:T(8,128)(2,1)S(1)}, u32[]{:S(2)}, u32[]{:S(2)}) async-start(bf16[16,16,512]{2,1,0:T(8,128)(2,1)} %reduce-scatter.3.cloned.1.call-done), calls=%async_computation.2 | async-start | bytes 524288 | tf_op jit(solution)/shard_map/all_to_all | solution.py:107
  184.8 13.4 %reduce-scatter.5.cloned.1.call-start = ((), (), s32[]{:S(2)}) async-start(), calls=%async_computation.5 | async-start | bytes 73728 | tf_op jit(solution)/shard_map/reduce_scatter | solution.py:118
Sparse Core Ops, SparseCore 0:
  166.0 13.1 reduce-scatter.2
  187.8 10.3 reduce-scatter.4
where the time goes:
time: 212 us
  other arithmetic  103 us (49%)
  blocking collectives  44.9 us (21%)
  waiting for transfers between devices  20.9 us (10%)
  between operations  13.6 us (6%)
  local copies, waits for them, and re-layouts  12.5 us (6%)
  matrix products  11.1 us (5%)
  starting transfers between devices  5.67 us (3%)
    another operation x2, other arithmetic  100 us
    all_to_all x1, blocking collectives, body(): lax.all_to_all(parcel, 'ep', split_axis=0, concat_axis=0, tiled=True)  16.3 us
    reduce_scatter x1, waiting for transfers between devices, body(): lax.psum_scatter(shared_term.astype(jnp.bfloat16), 'tp', scatter_dimensio...  12 us
    reduce_scatter x1, waiting for transfers between devices, body(): lax.psum_scatter(partial_value.astype(jnp.bfloat16), 'tp', scatter_dimens...  8.85 us
    all_gather x1, blocking collectives, body(): lax.all_gather(lax.all_to_all(parcel, 'ep', split_axis=0, concat_axis=0,...  8.77 us
    unnamed x39, local copies, waits for them, and re-layouts  7.58 us
    all_to_all x1, starting transfers between devices, body(): lax.all_to_all(summed, 'ep', split_axis=0, concat_axis=0, tiled=True)  5.63 us
    all_gather x1, blocking collectives, body(): lax.all_gather(mixed, 'tp', axis=0, tiled=True)  5.45 us
  transfers between devices with their start and end apart: 3, of which 2 were waited for; matrix products, arithmetic and copies ran while one was open for 1% of the time, Pallas kernels for 0%

commit v1 on v0

--- a/solution.py
+++ b/solution.py
@@ -1,7 +1,315 @@
+import functools
+
 import jax
 import jax.numpy as jnp
 from jax import lax
+from jax.experimental import pallas as pl
+from jax.experimental.pallas import tpu as pltpu
 from jax.sharding import PartitionSpec as P
+
+MESH = pl.DeviceIdType.MESH
+F32, BF16 = jnp.float32, jnp.bfloat16
+LANES = 128
+SEQ_BATCH = 5
+
+
+def kernel(
+    dims, resid, q, k_hbm, v_hbm, lens, offs, wout_h, g1, b1, routes, rw,
+    eg_h, eu_h, ed_h, sg_h, su_h, sd_h, g2, b2, out,
+    kb, vb, wout, eg, eu, ed, sg, su, sd,
+    qs, os_, rstage, reads, r24, sums1, cbuf, gath, hid, ysend, yown, sibin, zsend, xin, wsend, fin, sums2,
+    loc_sem, kv_sem, c_send, c_recv, cs_send, one_send, one_recv, ga_send, gx_send, gs_send, g_recv,
+    s1_send, s1_recv, s2_send, s2_recv, s3_send, s3_recv,
+):
+    ne, rows, rp, cols = dims
+    half = ne // 2
+    seqs, cache, kw = kb.shape
+    heads = offs.shape[0]
+    hd = q.shape[1] // heads
+    grouped = heads // (kw // hd)
+    nblk = cache // LANES
+    me, t = lax.axis_index("ep"), lax.axis_index("tp")
+    c, m = lax.rem(me, 2), me // 2
+    sib, peer = me + 1 - 2 * c, 1 - t
+    mine = c * half + m
+
+    def remote(src, dst, ss, rs, ep, tp):
+        return pltpu.make_async_remote_copy(
+            src_ref=src, dst_ref=dst, send_sem=ss, recv_sem=rs, device_id=(ep, tp), device_id_type=MESH
+        )
+
+    kv = []
+    for i in range(seqs):
+        kv.append((
+            pltpu.make_async_copy(k_hbm.at[i], kb.at[i], kv_sem.at[0, i]),
+            pltpu.make_async_copy(v_hbm.at[i], vb.at[i], kv_sem.at[1, i]),
+        ))
+    for lo in range(0, seqs, SEQ_BATCH):
+        for pair in kv[lo:lo + SEQ_BATCH]:
+            pair[0].start()
+        for pair in kv[lo:lo + SEQ_BATCH]:
+            pair[1].start()
+    weights = [
+        pltpu.make_async_copy(a, b, loc_sem.at[n])
+        for n, (a, b) in enumerate((
+            (wout_h, wout), (eg_h.at[0], eg), (eu_h.at[0], eu), (ed_h.at[0], ed), (sg_h, sg), (su_h, su), (sd_h, sd)
+        ))
+    ]
+    for copy in weights:
+        copy.start()
+
+    barrier = pltpu.get_barrier_semaphore()
+    for n in range(1, half):
+        pl.semaphore_signal(barrier, inc=1, device_id=(2 * lax.rem(m + n, half) + c, t), device_id_type=MESH)
+    pl.semaphore_signal(barrier, inc=1, device_id=(sib, t), device_id_type=MESH)
+    pl.semaphore_signal(barrier, inc=1, device_id=(me, peer), device_id_type=MESH)
+    pl.semaphore_wait(barrier, half + 1)
+
+    lane_r = lax.broadcasted_iota(jnp.int32, (rows, LANES), 1)
+    coef = jnp.zeros((rows, LANES), F32)
+    rt, wt = routes[...], rw[...]
+    for n in range(rt.shape[1]):
+        coef = coef + jnp.where(lane_r == rt[:, n:n + 1], wt[:, n:n + 1], 0.0)
+    cbuf[mine] = jnp.zeros((rp, LANES), F32)
+    cbuf[mine, 0:rows, :] = coef
+    c_copies = []
+    for n in range(1, half):
+        copy = remote(cbuf.at[mine], cbuf.at[mine], c_send.at[n - 1], c_recv.at[mine], 2 * lax.rem(m + n, half) + c, t)
+        copy.start()
+        c_copies.append(copy)
+
+    qf = q[...].astype(F32) * hd ** (-0.5)
+    lane_q = lax.broadcasted_iota(jnp.int32, (seqs, LANES), 1)
+    per = LANES // hd
+    for h in range(heads):
+        g = h // grouped
+        x = qf[:, LANES * (h // per):LANES * (h // per + 1)]
+        if h % per != g:
+            x = pltpu.roll(x, hd * ((g - h) % per), 1)
+        qs[:, h, :] = jnp.where(lane_q // hd == g, x, 0.0)
+    span = nblk * heads
+    row_i = lax.broadcasted_iota(jnp.int32, (span, LANES), 0)
+    pos = (row_i // heads) * LANES + lax.broadcasted_iota(jnp.int32, (span, LANES), 1)
+    off = jnp.zeros((span, LANES), F32)
+    for h in range(heads):
+        off = jnp.where(lax.rem(row_i, heads) == h, offs[h], off)
+    tri_r = lax.broadcasted_iota(jnp.int32, (LANES, 2 * LANES), 0)
+    tri_c = lax.broadcasted_iota(jnp.int32, (LANES, 2 * LANES), 1)
+    tri = jnp.where((tri_r > tri_c) | (tri_c >= LANES), 1.0, 0.0).astype(BF16)
+    for lo in range(0, seqs, SEQ_BATCH):
+        ids = range(lo, min(lo + SEQ_BATCH, seqs))
+        for i in ids:
+            kv[i][0].wait()
+        logs, keeps, lives = [], [], []
+        for i in ids:
+            sc = lax.dot_general(
+                qs[i].astype(BF16), kb[i], (((1,), (1,)), ((), ())), preferred_element_type=F32
+            )
+            s = jnp.concatenate([sc[:, LANES * j:LANES * (j + 1)] for j in range(nblk)], axis=0) - off
+            live = pos < lens[i]
+            tail = jnp.log(1.0 + jnp.exp(-jnp.abs(s)))
+            logs.append(jnp.minimum(s, 0.0) - tail)
+            keeps.append(jnp.where(live, -jnp.maximum(s, 0.0) - tail, 0.0))
+            lives.append(live)
+        keep = jnp.concatenate(keeps, axis=0)
+        hi = keep.astype(BF16)
+        low = (keep - hi.astype(F32)).astype(BF16)
+        sums = jnp.dot(hi, tri, preferred_element_type=F32) + jnp.dot(low, tri, preferred_element_type=F32)
+        for i in ids:
+            kv[i][1].wait()
+        for n, i in enumerate(ids):
+            acc = jnp.zeros((heads, LANES), F32)
+            parts = [None] * nblk
+            for j in reversed(range(nblk)):
+                a = n * span + j * heads
+                b = j * heads
+                w = jnp.exp(logs[n][b:b + heads] + sums[a:a + heads, :LANES] + acc)
+                parts[j] = jnp.where(lives[n][b:b + heads], w, 0.0)
+                acc = acc + sums[a:a + heads, LANES:]
+            os_[i] = jnp.dot(
+                jnp.concatenate(parts, axis=1).astype(BF16), vb[i], preferred_element_type=F32
+            )
+    rstage[...] = jnp.zeros_like(rstage)
+    for j in range(heads // per):
+        g = j * per // grouped
+        pick = jnp.zeros((seqs, LANES), F32)
+        for n in range(per):
+            x = os_[:, j * per + n, :]
+            if n != g:
+                x = pltpu.roll(x, hd * ((n - g) % per), 1)
+            pick = jnp.where(lane_q // hd == n, x, pick)
+        rstage[0:seqs, LANES * j:LANES * (j + 1)] = pick
+    reads[t] = rstage[...].astype(BF16)
+    rd = remote(reads.at[t], reads.at[t], one_send.at[0], one_recv.at[0], me, peer)
+    rd.start()
+    r24[...] = jnp.zeros_like(r24)
+    r24[0:rows, :] = resid[...].astype(F32) * 2.0**0.25
+    sp = reads.shape[1]
+    sel_r = lax.broadcasted_iota(jnp.int32, (rp, 2 * sp), 0)
+    sel_c = lax.broadcasted_iota(jnp.int32, (rp, 2 * sp), 1)
+    chosen = (sel_r == lax.rem(sel_c, sp) + seqs * (sel_c // sp)) & (lax.rem(sel_c, sp) < seqs)
+    select = jnp.where(chosen, 1.0, 0.0).astype(BF16)
+    weights[0].wait()
+    remote(reads.at[peer], reads.at[peer], one_send.at[0], one_recv.at[0], me, peer).wait_recv()
+    mixed = jnp.concatenate([reads[0], reads[1]], axis=0)
+    mixed = jnp.dot(select, mixed, preferred_element_type=F32).astype(BF16)
+    before = r24[...] + jnp.dot(mixed, wout[...], preferred_element_type=F32)
+
+    lane_s = lax.broadcasted_iota(jnp.int32, (rp, LANES), 1)
+
+    def exchange(buf, values, n):
+        total = jnp.sum(values, axis=1, keepdims=True)
+        square = jnp.sum(values * values, axis=1, keepdims=True)
+        buf[t] = jnp.where(lane_s == 0, total, square)
+        copy = remote(buf.at[t], buf.at[t], one_send.at[n], one_recv.at[n], me, peer)
+        copy.start()
+        remote(buf.at[peer], buf.at[peer], one_send.at[n], one_recv.at[n], me, peer).wait_recv()
+        both = buf[0] + buf[1]
+        centre = both[:, 0:1] / (2 * cols)
+        spread = both[:, 1:2] / (2 * cols) - centre * centre
+        return copy, centre, lax.rsqrt(spread + 1e-05)
+
+    sm1, centre, inv = exchange(sums1, before, 1)
+    normed = ((before - centre) * inv * g1[...] + b1[...]).astype(BF16)
+
+    gath[t, mine] = normed
+    copies = []
+
+    def send(copy):
+        copy.start()
+        copies.append(copy)
+
+    for n in range(1, half):
+        send(remote(gath.at[t, mine], gath.at[t, mine], ga_send.at[n - 1], g_recv.at[t, mine],
+                    2 * lax.rem(m + n, half) + c, t))
+    for n in range(half):
+        slot = c * half + lax.rem(m + half - n, half)
+        if n > 0:
+            remote(gath.at[t, slot], gath.at[t, slot], ga_send.at[0], g_recv.at[t, slot], me, peer).wait_recv()
+            remote(cbuf.at[slot], cbuf.at[slot], c_send.at[0], c_recv.at[slot], me, peer).wait_recv()
+        send(remote(gath.at[t, slot], gath.at[t, slot], gx_send.at[n], g_recv.at[t, slot], me, peer))
+        send(remote(gath.at[t, slot], gath.at[t, slot], gs_send.at[0, n], g_recv.at[t, slot], sib, t))
+        send(remote(cbuf.at[slot], cbuf.at[slot], cs_send.at[n], c_recv.at[slot], sib, t))
+    for n in range(half):
+        slot = c * half + lax.rem(m + half - n, half)
+        remote(gath.at[peer, slot], gath.at[peer, slot], ga_send.at[0], g_recv.at[peer, slot], me, peer).wait_recv()
+        send(remote(gath.at[peer, slot], gath.at[peer, slot], gs_send.at[1, n], g_recv.at[peer, slot], sib, t))
+    for copy in weights[1:]:
+        copy.wait()
+
+    def swiglu(x0, x1, wg, wu):
+        gp = jnp.dot(x0, wg[0:cols], preferred_element_type=F32) + jnp.dot(x1, wg[cols:], preferred_element_type=F32)
+        up = jnp.dot(x0, wu[0:cols], preferred_element_type=F32) + jnp.dot(x1, wu[cols:], preferred_element_type=F32)
+        return (gp * jax.nn.sigmoid(gp) * up).astype(BF16)
+
+    shared = jnp.dot(swiglu(gath[0, mine], gath[1, mine], sg, su), sd[...], preferred_element_type=F32)
+    own_rows, sib_rows = pl.ds(c * half, half), pl.ds((1 - c) * half, half)
+
+    def expert(which):
+        x0 = gath[0, which].reshape(half * rp, cols)
+        x1 = gath[1, which].reshape(half * rp, cols)
+        share = cbuf[which].reshape(half * rp, LANES)
+        lane = lax.broadcasted_iota(jnp.int32, (half * rp, LANES), 1)
+        share = jnp.sum(jnp.where(lane == me, share, 0.0), axis=1, keepdims=True)
+        hidden = swiglu(x0, x1, eg, eu)
+        return [
+            (jnp.dot(hidden, ed[:, cols * h:cols * (h + 1)], preferred_element_type=F32) * share).reshape(half, rp, cols)
+            for h in range(2)
+        ]
+
+    own = expert(own_rows)
+    yown[0], yown[1] = own[0], own[1]
+    yown[0, m] += shared[:, 0:cols]
+    yown[1, m] += shared[:, cols:]
+    for n in range(half):
+        slot = (1 - c) * half + n
+        for h in range(2):
+            remote(gath.at[h, slot], gath.at[h, slot], ga_send.at[0], g_recv.at[h, slot], me, peer).wait_recv()
+        remote(cbuf.at[slot], cbuf.at[slot], c_send.at[0], c_recv.at[slot], me, peer).wait_recv()
+    other = expert(sib_rows)
+    ysend[0], ysend[1] = other[0].astype(BF16), other[1].astype(BF16)
+    send(remote(ysend.at[peer], sibin.at[peer], s1_send.at[0], s1_recv.at[0], sib, t))
+    send(remote(ysend.at[t], sibin.at[t], s1_send.at[1], s1_recv.at[1], sib, t))
+    remote(ysend.at[peer], sibin.at[peer], s1_send.at[0], s1_recv.at[0], sib, t).wait_recv()
+    for n in range(half):
+        j = lax.rem(m + n + 1, half)
+        zsend[j] = (yown[peer, j] + sibin[peer, j].astype(F32)).astype(BF16)
+        send(remote(zsend.at[j], xin.at[j], s2_send.at[n], s2_recv.at[j], me, peer))
+    remote(ysend.at[t], sibin.at[t], s1_send.at[1], s1_recv.at[1], sib, t).wait_recv()
+    total = 2.0**0.25 * normed.astype(F32)
+    for n in range(half):
+        j = lax.rem(m + n + 1, half)
+        here = yown[t, j] + sibin[t, j].astype(F32)
+        remote(xin.at[j], xin.at[j], s2_send.at[0], s2_recv.at[j], me, peer).wait_recv()
+        here = here + xin[j].astype(F32)
+        if n < half - 1:
+            wsend[j] = here.astype(BF16)
+            send(remote(wsend.at[j], fin.at[m], s3_send.at[n], s3_recv.at[m], 2 * j + c, t))
+        else:
+            total = total + here
+    for n in range(1, half):
+        j = lax.rem(m + half - n, half)
+        remote(fin.at[j], fin.at[j], s3_send.at[0], s3_recv.at[j], me, peer).wait_recv()
+        total = total + fin[j].astype(F32)
+    sm2, centre, inv = exchange(sums2, total, 2)
+    final = (total - centre) * inv * g2[...] + b2[...]
+    out[...] = final[0:rows].astype(BF16)
+    for copy in c_copies + [rd, sm1, sm2] + copies:
+        copy.wait_send()
+
+
+def paired(ne, *args):
+    (resid, q, k, v, lens, offs, wout, g1, b1, routes, rw, eg, eu, ed, sg, su, sd, g2, b2) = args
+    rows, cols = resid.shape
+    rp = -(-rows // 8) * 8
+    half = ne // 2
+    seqs = q.shape[0]
+    sp = -(-seqs // 8) * 8
+    heads = offs.shape[0]
+    vm, anys, sm = (pl.BlockSpec(memory_space=s) for s in (pltpu.VMEM, pl.ANY, pltpu.SMEM))
+    dma = pltpu.SemaphoreType.DMA
+    return pl.pallas_call(
+        functools.partial(kernel, (ne, rows, rp, cols)),
+        out_shape=jax.ShapeDtypeStruct((rows, cols), BF16),
+        in_specs=[vm, vm, anys, anys, sm, sm, anys, vm, vm, vm, vm, anys, anys, anys, anys, anys, anys, vm, vm],
+        out_specs=vm,
+        scratch_shapes=[
+            pltpu.VMEM(k.shape, BF16),
+            pltpu.VMEM(v.shape, BF16),
+            pltpu.VMEM(wout.shape, BF16),
+            pltpu.VMEM(eg.shape[1:], BF16),
+            pltpu.VMEM(eu.shape[1:], BF16),
+            pltpu.VMEM(ed.shape[1:], BF16),
+            pltpu.VMEM(sg.shape, BF16),
+            pltpu.VMEM(su.shape, BF16),
+            pltpu.VMEM(sd.shape, BF16),
+            pltpu.VMEM((seqs, heads, LANES), F32),
+            pltpu.VMEM((seqs, heads, LANES), F32),
+            pltpu.VMEM((sp, q.shape[1]), F32),
+            pltpu.VMEM((2, sp, q.shape[1]), BF16),
+            pltpu.VMEM((rp, cols), F32),
+            pltpu.VMEM((2, rp, LANES), F32),
+            pltpu.VMEM((ne, rp, LANES), F32),
+            pltpu.VMEM((2, ne, rp, cols), BF16),
+            pltpu.VMEM((8, LANES), BF16),
+            pltpu.VMEM((2, half, rp, cols), BF16),
+            pltpu.VMEM((2, half, rp, cols), F32),
+            pltpu.VMEM((2, half, rp, cols), BF16),
+            pltpu.VMEM((half, rp, cols), BF16),
+            pltpu.VMEM((half, rp, cols), BF16),
+            pltpu.VMEM((half, rp, cols), BF16),
+            pltpu.VMEM((half, rp, cols), BF16),
+            pltpu.VMEM((2, rp, LANES), F32),
+            dma((7,)), dma((2, seqs)), dma((half,)), dma((ne,)), dma((half,)), dma((3,)), dma((3,)),
+            dma((half,)), dma((half,)), dma((2, half)), dma((2, ne)),
+            dma((2,)), dma((2,)), dma((half,)), dma((half,)), dma((half,)), dma((half,)),
+        ],
+        compiler_params=pltpu.CompilerParams(
+            collective_id=0, has_side_effects=True, vmem_limit_bytes=56 * 2**20
+        ),
+    )(resid, q, k, v, lens, offs, wout, g1.reshape(1, -1), b1.reshape(1, -1), routes, rw,
+      eg, eu, ed, sg, su, sd, g2.reshape(1, -1), b2.reshape(1, -1))
+
 
 H = 8
 HD = 64
@@ -150,4 +458,7 @@
         P("tp"),
     )
     out_specs = P("ep", "tp")
-    return jax.shard_map(body, mesh=mesh, in_specs=in_specs, out_specs=out_specs, check_vma=False)
+    ne = mesh.shape["ep"]
+    fits = mesh.shape["tp"] == 2 and ne % 2 == 0 and ne <= LANES // 4
+    step = functools.partial(paired, ne) if fits else body
+    return jax.shard_map(step, mesh=mesh, in_specs=in_specs, out_specs=out_specs, check_vma=False)

time: 212 us -> 44.9 us (0.21)
  other arithmetic: 103 us -> 0 us
  blocking collectives: 44.9 us -> 0 us
  Pallas kernels: 0 us -> 40.5 us
  waiting for transfers between devices: 20.9 us -> 0 us
  between operations: 13.6 us -> 0.01 us
  matrix products: 11.1 us -> 0 us
  local copies, waits for them, and re-layouts: 12.5 us -> 4.08 us
  starting transfers between devices: 5.67 us -> 0 us
    another operation x3 -> x0, other arithmetic: 101 us -> none
    pallas_call x0 -> x1, Pallas kernels: none -> 40.5 us  [paired(): pl.pallas_call(functools.partial(kernel, (ne, rows, rp, cols)), out_shape...]
    reduce_scatter x2 -> x0, waiting for transfers between devices: 20.9 us -> none  [the longest x1 12 us: body(): lax.psum_scatter(shared_term.astype(jnp.bfloat16), 'tp', scatter_dimensio...]
    all_gather x3 -> x0, blocking collectives: 18.7 us -> none  [the longest x1 8.77 us: body(): lax.all_gather(lax.all_to_all(parcel, 'ep', split_axis=0, concat_axis=0,...]
    all_to_all x1 -> x0, blocking collectives: 16.3 us -> none  [body(): lax.all_to_all(parcel, 'ep', split_axis=0, concat_axis=0, tiled=True)]
    dot_general x9 -> x0, matrix products: 11.1 us -> none  [the longest x1 3.29 us: stick_read(): jnp.einsum('sgjd,slgd->sgjl', query_heads, key_heads, preferred_element_t...]
    psum x2 -> x0, blocking collectives: 9.88 us -> none  [the longest x1 4.94 us: body(): lax.psum((jnp.sum(before, axis=1), jnp.sum(before * before, axis=1)), 'tp')]
    all_to_all x1 -> x0, starting transfers between devices: 5.63 us -> none  [body(): lax.all_to_all(summed, 'ep', split_axis=0, concat_axis=0, tiled=True)]
  transfers between devices with their start and end apart: 3 -> 0, of which waited for: 2 -> 0; matrix products, arithmetic and copies ran while one was open for 1% -> 0% of each run, Pallas kernels for 0% -> 0%
where the time goes in v1:
time: 44.9 us; the launch traced here: 44.6 us
  Pallas kernels  40.5 us (90%)
  local copies, waits for them, and re-layouts  4.08 us (9%)
    pallas_call x1, Pallas kernels, paired(): pl.pallas_call(functools.partial(kernel, (ne, rows, rp, cols)), out_shape...  40.5 us
    unnamed x3, local copies, waits for them, and re-layouts  4.08 us

profile of v1, /device:TPU:0, one launch (start us, length us, event | category | flops | bytes accessed | tf_op | source)
XLA Modules:
  0.0 44.6 jit_solution(10412091920450578581)
XLA Ops:
  0.0 1.4 %copy.20.routes = s32[20,6]{1,0:T(8,128)} copy(s32[20,6]{0,1:T(8,128)} %param.28) | data formatting | bytes 960 | tf_op args[9]
  1.4 1.4 %copy.21.rw = f32[20,6]{1,0:T(8,128)} copy(f32[20,6]{0,1:T(8,128)} %param.29) | data formatting | bytes 960 | tf_op args[10]
  2.7 40.5 %shard_map.181 = bf16[20,512]{1,0:T(8,128)(2,1)} custom-call(bf16[20,512]{1,0:T(8,128)(2,1)} %resid.1, bf16[10,512]{1,0:T(8,128)(2,1)} %q.1, bf16[10,1024,128]{2,1,0:T(8,128)(2,1)} %k_hbm.1, bf16[10,1024,128]{2,1,0:T(8,128)(2,1)} %v_hbm.1, s32[10]{0:T(128)} %lens.1, f32[8]{0:T(128)} %offs.1, bf16[512,512]{1,0:T(8,128)(2,1)} %wout_h.1, f32[1,512]{1,0:T(1,128)} %bitcast.4, ...), custom_call_target="tpu_custom_call" | custom-call | tf_op jit(solution)/shard_map/pallas_call | solution.py:271
  43.3 1.3 %copy.23 = bf16[20,512]{1,0:T(8,128)(2,1)} copy(bf16[20,512]{1,0:T(8,128)(2,1)} %shard_map.181) | data formatting | bytes 40960

commit v2 on v1

--- a/solution.py
+++ b/solution.py
@@ -10,14 +10,15 @@
 MESH = pl.DeviceIdType.MESH
 F32, BF16 = jnp.float32, jnp.bfloat16
 LANES = 128
-SEQ_BATCH = 5
+SEQ_BATCH = 10
 
 
 def kernel(
-    dims, resid, q, k_hbm, v_hbm, lens, offs, wout_h, g1, b1, routes, rw,
-    eg_h, eu_h, ed_h, sg_h, su_h, sd_h, g2, b2, out,
+    dims, resid_h, q_h, k_hbm, v_hbm, lens, offs, wout_h, g1_h, b1_h, routes_h, rw_h,
+    eg_h, eu_h, ed_h, sg_h, su_h, sd_h, g2_h, b2_h, out,
+    resid, q, g1, b1, routes, rw, g2, b2, rpad, wpad, small_sem,
     kb, vb, wout, eg, eu, ed, sg, su, sd,
-    qs, os_, rstage, reads, r24, sums1, cbuf, gath, hid, ysend, yown, sibin, zsend, xin, wsend, fin, sums2,
+    qs, os_, rstage, reads, r24, sums1, cbuf, gath, ysend, yown, sibin, zsend, xin, wsend, fin, sums2,
     loc_sem, kv_sem, c_send, c_recv, cs_send, one_send, one_recv, ga_send, gx_send, gs_send, g_recv,
     s1_send, s1_recv, s2_send, s2_recv, s3_send, s3_recv,
 ):
@@ -31,6 +32,15 @@
     me, t = lax.axis_index("ep"), lax.axis_index("tp")
     c, m = lax.rem(me, 2), me // 2
     sib, peer = me + 1 - 2 * c, 1 - t
+
+    def mate(n):
+        j, bit = 0, 1
+        while bit < half:
+            b = lax.rem(m // bit, 2)
+            j = j + bit * ((1 - b) if n & bit else b)
+            bit *= 2
+        return j
+
     mine = c * half + m
 
     def remote(src, dst, ss, rs, ep, tp):
@@ -38,6 +48,20 @@
             src_ref=src, dst_ref=dst, send_sem=ss, recv_sem=rs, device_id=(ep, tp), device_id_type=MESH
         )
 
+    barrier = pltpu.get_barrier_semaphore()
+    for n in range(1, half):
+        pl.semaphore_signal(barrier, inc=1, device_id=(2 * mate(n) + c, t), device_id_type=MESH)
+    pl.semaphore_signal(barrier, inc=1, device_id=(sib, t), device_id_type=MESH)
+    pl.semaphore_signal(barrier, inc=1, device_id=(me, peer), device_id_type=MESH)
+
+    small = [
+        pltpu.make_async_copy(a, b, small_sem.at[n])
+        for n, (a, b) in enumerate((
+            (routes_h, routes), (rw_h, rw), (q_h, q), (resid_h, resid), (g1_h, g1), (b1_h, b1), (g2_h, g2), (b2_h, b2)
+        ))
+    ]
+    for copy in small:
+        copy.start()
     kv = []
     for i in range(seqs):
         kv.append((
@@ -58,26 +82,8 @@
     for copy in weights:
         copy.start()
 
-    barrier = pltpu.get_barrier_semaphore()
-    for n in range(1, half):
-        pl.semaphore_signal(barrier, inc=1, device_id=(2 * lax.rem(m + n, half) + c, t), device_id_type=MESH)
-    pl.semaphore_signal(barrier, inc=1, device_id=(sib, t), device_id_type=MESH)
-    pl.semaphore_signal(barrier, inc=1, device_id=(me, peer), device_id_type=MESH)
-    pl.semaphore_wait(barrier, half + 1)
-
-    lane_r = lax.broadcasted_iota(jnp.int32, (rows, LANES), 1)
-    coef = jnp.zeros((rows, LANES), F32)
-    rt, wt = routes[...], rw[...]
-    for n in range(rt.shape[1]):
-        coef = coef + jnp.where(lane_r == rt[:, n:n + 1], wt[:, n:n + 1], 0.0)
-    cbuf[mine] = jnp.zeros((rp, LANES), F32)
-    cbuf[mine, 0:rows, :] = coef
-    c_copies = []
-    for n in range(1, half):
-        copy = remote(cbuf.at[mine], cbuf.at[mine], c_send.at[n - 1], c_recv.at[mine], 2 * lax.rem(m + n, half) + c, t)
-        copy.start()
-        c_copies.append(copy)
-
+
+    small[2].wait()
     qf = q[...].astype(F32) * hd ** (-0.5)
     lane_q = lax.broadcasted_iota(jnp.int32, (seqs, LANES), 1)
     per = LANES // hd
@@ -139,9 +145,28 @@
                 x = pltpu.roll(x, hd * ((n - g) % per), 1)
             pick = jnp.where(lane_q // hd == n, x, pick)
         rstage[0:seqs, LANES * j:LANES * (j + 1)] = pick
+    for copy in small[:2] + small[3:]:
+        copy.wait()
+    expert_of = lax.broadcasted_iota(jnp.int32, (LANES, LANES), 0)
+    coef = jnp.zeros((LANES, LANES), F32)
+    topk = routes.shape[0]
+    rpad[...] = jnp.full(rpad.shape, -1, jnp.int32)
+    wpad[...] = jnp.zeros(wpad.shape, F32)
+    rpad[0:topk, 0:rows] = routes[...]
+    wpad[0:topk, 0:rows] = rw[...]
+    rt, wt = rpad[...], wpad[...]
+    for n in range(topk):
+        coef = coef + jnp.where(expert_of == rt[n:n + 1, :], wt[n:n + 1, :], 0.0)
+    cbuf[mine] = coef.T[0:rp]
+    pl.semaphore_wait(barrier, half + 1)
     reads[t] = rstage[...].astype(BF16)
     rd = remote(reads.at[t], reads.at[t], one_send.at[0], one_recv.at[0], me, peer)
     rd.start()
+    c_copies = []
+    for n in range(1, half):
+        copy = remote(cbuf.at[mine], cbuf.at[mine], c_send.at[n - 1], c_recv.at[mine], 2 * mate(n) + c, t)
+        copy.start()
+        c_copies.append(copy)
     r24[...] = jnp.zeros_like(r24)
     r24[0:rows, :] = resid[...].astype(F32) * 2.0**0.25
     sp = reads.shape[1]
@@ -181,9 +206,9 @@
 
     for n in range(1, half):
         send(remote(gath.at[t, mine], gath.at[t, mine], ga_send.at[n - 1], g_recv.at[t, mine],
-                    2 * lax.rem(m + n, half) + c, t))
+                    2 * mate(n) + c, t))
     for n in range(half):
-        slot = c * half + lax.rem(m + half - n, half)
+        slot = c * half + mate(n)
         if n > 0:
             remote(gath.at[t, slot], gath.at[t, slot], ga_send.at[0], g_recv.at[t, slot], me, peer).wait_recv()
             remote(cbuf.at[slot], cbuf.at[slot], c_send.at[0], c_recv.at[slot], me, peer).wait_recv()
@@ -191,7 +216,7 @@
         send(remote(gath.at[t, slot], gath.at[t, slot], gs_send.at[0, n], g_recv.at[t, slot], sib, t))
         send(remote(cbuf.at[slot], cbuf.at[slot], cs_send.at[n], c_recv.at[slot], sib, t))
     for n in range(half):
-        slot = c * half + lax.rem(m + half - n, half)
+        slot = c * half + mate(n)
         remote(gath.at[peer, slot], gath.at[peer, slot], ga_send.at[0], g_recv.at[peer, slot], me, peer).wait_recv()
         send(remote(gath.at[peer, slot], gath.at[peer, slot], gs_send.at[1, n], g_recv.at[peer, slot], sib, t))
     for copy in weights[1:]:
@@ -203,52 +228,58 @@
         return (gp * jax.nn.sigmoid(gp) * up).astype(BF16)
 
     shared = jnp.dot(swiglu(gath[0, mine], gath[1, mine], sg, su), sd[...], preferred_element_type=F32)
-    own_rows, sib_rows = pl.ds(c * half, half), pl.ds((1 - c) * half, half)
-
-    def expert(which):
-        x0 = gath[0, which].reshape(half * rp, cols)
-        x1 = gath[1, which].reshape(half * rp, cols)
-        share = cbuf[which].reshape(half * rp, LANES)
-        lane = lax.broadcasted_iota(jnp.int32, (half * rp, LANES), 1)
+    def expert(slots):
+        def rows_of(buf):
+            return jnp.concatenate([buf[s] for s in slots], axis=0)
+
+        share = rows_of(cbuf)
+        lane = lax.broadcasted_iota(jnp.int32, share.shape, 1)
         share = jnp.sum(jnp.where(lane == me, share, 0.0), axis=1, keepdims=True)
-        hidden = swiglu(x0, x1, eg, eu)
-        return [
-            (jnp.dot(hidden, ed[:, cols * h:cols * (h + 1)], preferred_element_type=F32) * share).reshape(half, rp, cols)
-            for h in range(2)
-        ]
-
-    own = expert(own_rows)
-    yown[0], yown[1] = own[0], own[1]
+        hidden = swiglu(rows_of(gath.at[0]), rows_of(gath.at[1]), eg, eu)
+        for h in (peer, t):
+            part = jnp.dot(hidden, ed[:, pl.ds(pl.multiple_of(h * cols, cols), cols)], preferred_element_type=F32)
+            yield h, (part * share).reshape(len(slots), rp, cols)
+
+    order = [mate(n) for n in reversed(range(half))]
+    for h, part in expert([c * half + n for n in range(half)]):
+        yown[h] = part
     yown[0, m] += shared[:, 0:cols]
     yown[1, m] += shared[:, cols:]
-    for n in range(half):
-        slot = (1 - c) * half + n
-        for h in range(2):
-            remote(gath.at[h, slot], gath.at[h, slot], ga_send.at[0], g_recv.at[h, slot], me, peer).wait_recv()
-        remote(cbuf.at[slot], cbuf.at[slot], c_send.at[0], c_recv.at[slot], me, peer).wait_recv()
-    other = expert(sib_rows)
-    ysend[0], ysend[1] = other[0].astype(BF16), other[1].astype(BF16)
-    send(remote(ysend.at[peer], sibin.at[peer], s1_send.at[0], s1_recv.at[0], sib, t))
-    send(remote(ysend.at[t], sibin.at[t], s1_send.at[1], s1_recv.at[1], sib, t))
-    remote(ysend.at[peer], sibin.at[peer], s1_send.at[0], s1_recv.at[0], sib, t).wait_recv()
-    for n in range(half):
-        j = lax.rem(m + n + 1, half)
-        zsend[j] = (yown[peer, j] + sibin[peer, j].astype(F32)).astype(BF16)
-        send(remote(zsend.at[j], xin.at[j], s2_send.at[n], s2_recv.at[j], me, peer))
-    remote(ysend.at[t], sibin.at[t], s1_send.at[1], s1_recv.at[1], sib, t).wait_recv()
+    cut = (half + 1) // 2
+    for part_id, (lo, hi) in enumerate(((0, cut), (cut, half))):
+        slots = [(1 - c) * half + j for j in order[lo:hi]]
+        for slot in slots:
+            for h in range(2):
+                remote(gath.at[h, slot], gath.at[h, slot], ga_send.at[0], g_recv.at[h, slot], me, peer).wait_recv()
+            remote(cbuf.at[slot], cbuf.at[slot], c_send.at[0], c_recv.at[slot], me, peer).wait_recv()
+        for half_id, (h, part) in enumerate(expert(slots)):
+            ysend[h, lo:hi] = part.astype(BF16)
+            send(remote(ysend.at[h, pl.ds(lo, hi - lo)], sibin.at[h, pl.ds(lo, hi - lo)],
+                        s1_send.at[half_id, part_id], s1_recv.at[half_id, part_id], sib, t))
+
+    def arrived(half_id, h, n):
+        for part_id, (lo, hi) in enumerate(((0, cut), (cut, half))):
+            if n == lo:
+                ref = sibin.at[h, pl.ds(lo, hi - lo)]
+                remote(ref, ref, s1_send.at[0, 0], s1_recv.at[half_id, part_id], sib, t).wait_recv()
+
+    for n, j in enumerate(order):
+        arrived(0, peer, n)
+        zsend[n] = (yown[peer, j] + sibin[peer, n].astype(F32)).astype(BF16)
+        send(remote(zsend.at[n], xin.at[n], s2_send.at[n], s2_recv.at[n], me, peer))
     total = 2.0**0.25 * normed.astype(F32)
-    for n in range(half):
-        j = lax.rem(m + n + 1, half)
-        here = yown[t, j] + sibin[t, j].astype(F32)
-        remote(xin.at[j], xin.at[j], s2_send.at[0], s2_recv.at[j], me, peer).wait_recv()
-        here = here + xin[j].astype(F32)
+    for n, j in enumerate(order):
+        arrived(1, t, n)
+        here = yown[t, j] + sibin[t, n].astype(F32)
+        remote(xin.at[n], xin.at[n], s2_send.at[0], s2_recv.at[n], me, peer).wait_recv()
+        here = here + xin[n].astype(F32)
         if n < half - 1:
-            wsend[j] = here.astype(BF16)
-            send(remote(wsend.at[j], fin.at[m], s3_send.at[n], s3_recv.at[m], 2 * j + c, t))
+            wsend[n] = here.astype(BF16)
+            send(remote(wsend.at[n], fin.at[m], s3_send.at[n], s3_recv.at[m], 2 * j + c, t))
         else:
             total = total + here
     for n in range(1, half):
-        j = lax.rem(m + half - n, half)
+        j = mate(n)
         remote(fin.at[j], fin.at[j], s3_send.at[0], s3_recv.at[j], me, peer).wait_recv()
         total = total + fin[j].astype(F32)
     sm2, centre, inv = exchange(sums2, total, 2)
@@ -271,9 +302,20 @@
     return pl.pallas_call(
         functools.partial(kernel, (ne, rows, rp, cols)),
         out_shape=jax.ShapeDtypeStruct((rows, cols), BF16),
-        in_specs=[vm, vm, anys, anys, sm, sm, anys, vm, vm, vm, vm, anys, anys, anys, anys, anys, anys, vm, vm],
+        in_specs=[anys] * 4 + [sm] * 2 + [anys] * 13,
         out_specs=vm,
         scratch_shapes=[
+            pltpu.VMEM(resid.shape, BF16),
+            pltpu.VMEM(q.shape, BF16),
+            pltpu.VMEM((1, cols), F32),
+            pltpu.VMEM((1, cols), F32),
+            pltpu.VMEM(routes.shape[::-1], jnp.int32),
+            pltpu.VMEM(rw.shape[::-1], F32),
+            pltpu.VMEM((1, cols), F32),
+            pltpu.VMEM((1, cols), F32),
+            pltpu.VMEM((-(-routes.shape[1] // 8) * 8, LANES), jnp.int32),
+            pltpu.VMEM((-(-routes.shape[1] // 8) * 8, LANES), F32),
+            dma((8,)),
             pltpu.VMEM(k.shape, BF16),
             pltpu.VMEM(v.shape, BF16),
             pltpu.VMEM(wout.shape, BF16),
@@ -291,7 +333,6 @@
             pltpu.VMEM((2, rp, LANES), F32),
             pltpu.VMEM((ne, rp, LANES), F32),
             pltpu.VMEM((2, ne, rp, cols), BF16),
-            pltpu.VMEM((8, LANES), BF16),
             pltpu.VMEM((2, half, rp, cols), BF16),
             pltpu.VMEM((2, half, rp, cols), F32),
             pltpu.VMEM((2, half, rp, cols), BF16),
@@ -302,12 +343,12 @@
             pltpu.VMEM((2, rp, LANES), F32),
             dma((7,)), dma((2, seqs)), dma((half,)), dma((ne,)), dma((half,)), dma((3,)), dma((3,)),
             dma((half,)), dma((half,)), dma((2, half)), dma((2, ne)),
-            dma((2,)), dma((2,)), dma((half,)), dma((half,)), dma((half,)), dma((half,)),
+            dma((2, 2)), dma((2, 2)), dma((half,)), dma((half,)), dma((half,)), dma((half,)),
         ],
         compiler_params=pltpu.CompilerParams(
             collective_id=0, has_side_effects=True, vmem_limit_bytes=56 * 2**20
         ),
-    )(resid, q, k, v, lens, offs, wout, g1.reshape(1, -1), b1.reshape(1, -1), routes, rw,
+    )(resid, q, k, v, lens, offs, wout, g1.reshape(1, -1), b1.reshape(1, -1), routes.T, rw.T,
       eg, eu, ed, sg, su, sd, g2.reshape(1, -1), b2.reshape(1, -1))
 
 
@@ -459,6 +500,6 @@
     )
     out_specs = P("ep", "tp")
     ne = mesh.shape["ep"]
-    fits = mesh.shape["tp"] == 2 and ne % 2 == 0 and ne <= LANES // 4
+    fits = mesh.shape["tp"] == 2 and ne in (2, 4, 8, 16, 32)
     step = functools.partial(paired, ne) if fits else body
     return jax.shard_map(step, mesh=mesh, in_specs=in_specs, out_specs=out_specs, check_vma=False)

time: 44.9 us -> 41.1 us (0.915)
  local copies, waits for them, and re-layouts: 4.08 us -> 1.35 us
  Pallas kernels: 40.5 us -> 39.6 us
    unnamed x3 -> x1, local copies, waits for them, and re-layouts: 4.08 us -> 1.35 us
    pallas_call x1, Pallas kernels: 40.5 us -> 39.6 us  [paired(): pl.pallas_call(functools.partial(kernel, (ne, rows, rp, cols)), out_shape...]
where the time goes in v2:
time: 41.1 us; the launch traced here: 40.9 us
  Pallas kernels  39.6 us (96%)
  local copies, waits for them, and re-layouts  1.35 us (3%)
    pallas_call x1, Pallas kernels, paired(): pl.pallas_call(functools.partial(kernel, (ne, rows, rp, cols)), out_shape...  39.6 us
    unnamed x1, local copies, waits for them, and re-layouts  1.35 us

profile of v2, /device:TPU:0, one launch (start us, length us, event | category | flops | bytes accessed | tf_op | source)
XLA Modules:
  0.0 40.9 jit_solution(16641748472649289247)
XLA Ops:
  0.0 39.6 %shard_map.181 = bf16[20,512]{1,0:T(8,128)(2,1)} custom-call(bf16[20,512]{1,0:T(8,128)(2,1)} %resid_h.1, bf16[10,512]{1,0:T(8,128)(2,1)} %q_h.1, bf16[10,1024,128]{2,1,0:T(8,128)(2,1)} %k_hbm.1, bf16[10,1024,128]{2,1,0:T(8,128)(2,1)} %v_hbm.1, s32[10]{0:T(128)} %lens.1, f32[8]{0:T(128)} %offs.1, bf16[512,512]{1,0:T(8,128)(2,1)} %wout_h.1, f32[1,512]{1,0:T(1,128)} %bitcast.8, ...), custom_call_target="tpu_custom_call" | custom-call | tf_op jit(solution)/shard_map/pallas_call | solution.py:302
  39.6 1.3 %copy.21 = bf16[20,512]{1,0:T(8,128)(2,1)} copy(bf16[20,512]{1,0:T(8,128)(2,1)} %shard_map.181) | data formatting | bytes 40960
